TPU v7x, 32 devices: a whole 2x2x4 slice. The times are simulated.
32 devices in a mesh: sp: 4 (over z), fs: 4 (over y, x), tp: 2 (over core).
Axes of the slice: x: 2, y: 2, z: 4, core: 2. Of those that a mesh axis runs over, the one named last changes fastest.
Arguments:
- inputs: bfloat16 [4, 2048, 2048], P('fs', 'sp', 'tp'), may hold values from -6 to 6
- norm_gain: float32 [2048], replicated, may hold values from 0.1 to 1.9
- query_weight: bfloat16 [2048, 1024], P(('sp', 'fs'), 'tp'), may hold values from -0.125 to 0.125
- key_weight: bfloat16 [2048, 1024], P(('sp', 'fs'), 'tp'), may hold values from -0.125 to 0.125
- value_weight: bfloat16 [2048, 1024], P(('sp', 'fs'), 'tp'), may hold values from -0.125 to 0.125
- query_gain: float32 [64], replicated, may hold values from 0.8 to 7
- key_gain: float32 [64], replicated, may hold values from 0.8 to 7
- mix_lambda: float32 [8], replicated, may hold values from 0.3 to 0.8
- head_gain: float32 [128], replicated, may hold values from 0.1 to 1.9
- post_gate_weight: bfloat16 [2048, 2048], P(('sp', 'fs'), 'tp'), may hold values from -0.125 to 0.125
- pre_gate_weight: bfloat16 [2048, 2048], P(('sp', 'fs'), 'tp'), may hold values from -0.125 to 0.125
- inner_weight: bfloat16 [2048, 2048], P(('sp', 'fs'), 'tp'), may hold values from -0.125 to 0.125
- conv_taps: float32 [3, 2048], replicated, may hold values from -3 to 3
- attn_out_weight: bfloat16 [2048, 1024], P(('sp', 'fs'), 'tp'), may hold values from -0.109375 to 0.109375
- conv_out_weight: bfloat16 [2048, 2048], P(('sp', 'fs'), 'tp'), may hold values from -0.109375 to 0.109375
Outputs:
- mixed: bfloat16 [4, 2048, 2048], P('fs', ('sp', 'tp'))
All inputs are finite; a program needn't handle non-finite values.
Results may differ from a plain program's by a relative error of at most 0.015.
The roundings to bfloat16 on the way count: a program that leaves them out, or rounds other values in their place, can miss the bound.
Values may be sent and summed in bfloat16 or wider, within the bound.
A program may use at most 128 MiB of HBM per device.

v0:
```python
import math

import jax
import jax.numpy as jnp
from jax import lax
from jax.sharding import PartitionSpec as P

epsilon = 1e-06


def padded_2(x, sides, width):
    for axis, dim in sides:
        size, length = (lax.axis_size(axis), x.shape[dim])
        up = [(i, (i + 1) % size) for i in range(size - 1)]
        down = [(j, i) for i, j in up]
        last = lax.slice_in_dim(x, length - width, length, axis=dim)
        initial = lax.slice_in_dim(x, 0, width, axis=dim)
        before = lax.ppermute(last, axis, up)
        after = lax.ppermute(initial, axis, down)
        x = jnp.concatenate([before, x, after], axis=dim)
    return x


def scale_rows(values, gain):
    return values * lax.rsqrt(jnp.mean(values * values, axis=-1, keepdims=True) + epsilon) * gain


def project_all(normed, weights, products):
    result = []
    for member in range(len(weights)):
        if member < products:
            result.append(jnp.dot(normed, weights[member], preferred_element_type=jnp.float32))
        else:
            result.append(weights[member])
    return tuple(result)


def attention_branch(query, key, values, weight_two, query_gain, key_gain, head_gain):
    tok_rows = query.shape[0]
    vsize = head_gain.shape[0]
    half = query_gain.shape[0]
    heads = values.shape[1] // vsize
    query_normed = scale_rows(query.reshape(tok_rows, heads, 2, half), query_gain).astype(
        jnp.bfloat16
    )
    key_normed = scale_rows(key.reshape(tok_rows, heads * 2, half), key_gain).astype(jnp.bfloat16)
    key_normed = key_normed.reshape(tok_rows, heads * 2 * half)
    scale = half ** (-0.5)
    initial = (
        jnp.full((heads, 2, tok_rows), -1e30, jnp.float32),
        jnp.zeros((heads, 2, tok_rows), jnp.float32),
        jnp.zeros((heads, 2, tok_rows, vsize), jnp.float32),
    )
    carry = initial
    key_piece = lax.all_gather(key_normed, "sp", axis=0, tiled=True)
    value_piece = lax.all_gather(values, "sp", axis=0, tiled=True)
    length = key_piece.shape[0]
    block = math.gcd(length, 512)
    key_blocks = key_piece.reshape(length // block, block, heads, 2, half)
    value_blocks = value_piece.reshape(length // block, block, heads, vsize)

    def one_block(state, blocks):
        peak, total, accum = state
        key_block, value_block = blocks
        scores = (
            jnp.einsum(
                "qhjd,khjd->hjqk", query_normed, key_block, preferred_element_type=jnp.float32
            )
            * scale
        )
        new_peak = jnp.maximum(peak, jnp.max(scores, axis=-1))
        factor = jnp.exp(peak - new_peak)
        expo = jnp.exp(scores - new_peak[..., None])
        total = total * factor + jnp.sum(expo, axis=-1)
        accum = accum * factor[..., None] + jnp.einsum(
            "hjqk,khd->hjqd",
            expo.astype(jnp.bfloat16),
            value_block,
            preferred_element_type=jnp.float32,
        )
        return ((new_peak, total, accum), None)

    carry, unused = lax.scan(one_block, carry, (key_blocks, value_blocks))
    peak, total, accum = carry
    mapped = accum / total[..., None]
    head_out = mapped[:, 0] - weight_two[:, None, None] * mapped[:, 1]
    normed_out = scale_rows(head_out, head_gain).astype(jnp.bfloat16)
    return jnp.transpose(normed_out, (1, 0, 2)).reshape(tok_rows, heads * vsize)


def per_device(
    inputs,
    norm_gain,
    query_weight,
    key_weight,
    value_weight,
    query_gain,
    key_gain,
    mix_lambda,
    head_gain,
    post_gate_weight,
    pre_gate_weight,
    inner_weight,
    conv_taps,
    attn_out_weight,
    conv_out_weight,
):
    tokens = inputs[0]
    whole = lax.all_gather(tokens, "tp", axis=1, tiled=True)
    normed = scale_rows(whole.astype(jnp.float32), norm_gain).astype(jnp.bfloat16)
    heads_dev = value_weight.shape[1] // head_gain.shape[0]
    channels = post_gate_weight.shape[1]
    tp_index = lax.axis_index("tp")
    weight_two = lax.dynamic_slice_in_dim(mix_lambda, tp_index * heads_dev, heads_dev)
    taps = lax.dynamic_slice_in_dim(conv_taps, tp_index * channels, channels, 1)
    every_full = (
        lax.all_gather(query_weight, ("sp", "fs"), axis=0, tiled=True),
        lax.all_gather(key_weight, ("sp", "fs"), axis=0, tiled=True),
        lax.all_gather(value_weight, ("sp", "fs"), axis=0, tiled=True),
        lax.all_gather(post_gate_weight, ("sp", "fs"), axis=0, tiled=True),
        lax.all_gather(pre_gate_weight, ("sp", "fs"), axis=0, tiled=True),
        lax.all_gather(inner_weight, ("sp", "fs"), axis=0, tiled=True),
        lax.all_gather(attn_out_weight, ("sp", "fs"), axis=0, tiled=True),
        lax.all_gather(conv_out_weight, ("sp", "fs"), axis=0, tiled=True),
    )
    query, key, value_proj, post, pre_gate, inner, attn_out_full, conv_out_full = project_all(
        normed, every_full[0:3] + every_full[3:6] + every_full[6:8], 6
    )
    attn_hidden = attention_branch(
        query, key, value_proj.astype(jnp.bfloat16), weight_two, query_gain, key_gain, head_gain
    )
    post_mid = post.astype(jnp.bfloat16)
    post_wide = lax.optimization_barrier(post_mid).astype(jnp.float32)
    signal = (pre_gate * inner).astype(jnp.bfloat16)
    padded = padded_2(signal, (("sp", 0),), 1)
    shifted = lax.optimization_barrier(padded).astype(jnp.float32)
    filtered = taps[0] * shifted[:-2] + taps[1] * shifted[1:-1] + taps[2] * shifted[2:]
    conv_hidden = (post_wide * filtered).astype(jnp.bfloat16)
    contract = (((1,), (1,)), ((), ()))
    summed = lax.psum_scatter(
        (
            lax.dot_general(
                attn_hidden, attn_out_full, contract, preferred_element_type=jnp.float32
            )
            + lax.dot_general(
                conv_hidden, conv_out_full, contract, preferred_element_type=jnp.float32
            )
        ).astype(jnp.bfloat16),
        "tp",
        scatter_dimension=0,
        tiled=True,
    )
    return summed[None]


def solution(mesh):
    placed = (
        P("fs", "sp", "tp"),
        P(),
        P(("sp", "fs"), "tp"),
        P(("sp", "fs"), "tp"),
        P(("sp", "fs"), "tp"),
        P(),
        P(),
        P(),
        P(),
        P(("sp", "fs"), "tp"),
        P(("sp", "fs"), "tp"),
        P(("sp", "fs"), "tp"),
        P(),
        P(("sp", "fs"), "tp"),
        P(("sp", "fs"), "tp"),
    )
    return jax.shard_map(
        per_device,
        mesh=mesh,
        in_specs=placed,
        out_specs=P("fs", ("sp", "tp"), None),
        check_vma=False,
    )
```

profile of v0, /device:TPU:9, one launch (start us, length us, event | category | flops | bytes accessed | tf_op | source)
XLA Modules:
  0.0 692.2 jit_solution(11032667689516088220)
XLA Ops:
  10.1 11.3 %all-gather.33.cloned.1.call-done = bf16[1,512,2048]{2,1,0:T(8,128)(2,1)} async-done(((bf16[1,512,1024]{2,1,0:T(8,128)(2,1)}), bf16[1,512,2048]{2,1,0:T(8,128)(2,1)}) %all-gather.33.cloned.1.call-update) | async-done | bytes 2097168 | tf_op jit(solution)/shard_map/all_gather | solution.py:109
  21.4 2.2 fusion.17
  23.6 60.4 %all-gather.13.cloned.1.call-done = bf16[2048,512]{1,0:T(8,128)(2,1)} async-done(((bf16[128,512]{1,0:T(8,128)(2,1)}), bf16[2048,512]{1,0:T(8,128)(2,1)}) %all-gather.13.cloned.1.call-update) | async-done | bytes 2097168 | tf_op jit(solution)/shard_map/all_gather | solution.py:118
  84.0 3.0 bitcast_reduce_fusion.1
  87.0 1.0 fusion.29
  88.1 57.9 %all-gather.19.cloned.1.call-done = bf16[2048,512]{1,0:T(8,128)(2,1)} async-done(((bf16[128,512]{1,0:T(8,128)(2,1)}), bf16[2048,512]{1,0:T(8,128)(2,1)}) %all-gather.19.cloned.1.call-update) | async-done | bytes 2097168 | tf_op jit(solution)/shard_map/all_gather | solution.py:119
  146.0 3.7 convolution_convert_fusion.1
  153.6 0.9 constant_dynamic-slice_fusion.1
  154.6 53.3 %all-gather.17.cloned.1.call-done = bf16[2048,512]{1,0:T(8,128)(2,1)} async-done(((bf16[128,512]{1,0:T(8,128)(2,1)}), bf16[2048,512]{1,0:T(8,128)(2,1)}) %all-gather.17.cloned.1.call-update) | async-done | bytes 2097168 | tf_op jit(solution)/shard_map/all_gather | solution.py:117
  207.9 3.6 multiply_reduce_fusion.1
  211.8 41.2 %all-gather.15.cloned.1.call-done = bf16[2048,512]{0,1:T(8,128)(2,1)} async-done(((bf16[512,512]{0,1:T(8,128)(2,1)}), bf16[2048,512]{0,1:T(8,128)(2,1)}) %all-gather.15.cloned.1.call-update) | async-done | bytes 2097168 | tf_op jit(solution)/shard_map/all_gather | solution.py:55
  252.9 4.5 reshape.57
  257.4 3.4 copy.21
  260.8 38.0 %all-gather.21.cloned.1.call-done = bf16[2048,512]{1,0:T(8,128)(2,1)} async-done(((bf16[512,512]{1,0:T(8,128)(2,1)}), bf16[2048,512]{1,0:T(8,128)(2,1)}) %all-gather.21.cloned.1.call-update) | async-done | bytes 2097168 | tf_op jit(solution)/shard_map/all_gather | solution.py:56
  298.8 4.0 reshape.59
  302.8 59.3 %while.15 = (s32[]{:T(128)}, f32[4,2,512]{2,1,0:T(2,128)S(1)}, f32[4,2,512]{2,1,0:T(2,128)S(1)}, f32[4,2,512,128]{3,2,1,0:T(8,128)S(1)}, bf16[4,512,4,2,64]{1,4,...) while((s32[]{:T(128)}, f32[4,2,512]{2,1,0:T(2,128)S(1)}, ...), condition=%wide.region_6.7_spmd.clone, body=%wide.region_3.6_spmd.clone.sunk | while | flops 823676928 | bytes 65798792 | solution.py:83
  302.8 5.6 bitcast_reduce_fusion.3
  308.5 5.1 fusion.62
  313.7 1.2 constant_dynamic-slice_fusion.3
  314.9 2.8 fusion.64
  317.7 5.6 bitcast_reduce_fusion.3
  323.4 5.0 fusion.62
  328.4 1.3 constant_dynamic-slice_fusion.3
  329.7 2.8 fusion.64
  332.5 5.6 bitcast_reduce_fusion.3
  338.2 5.0 fusion.62
  343.2 1.2 constant_dynamic-slice_fusion.3
  344.5 2.8 fusion.64
  347.3 5.7 bitcast_reduce_fusion.3
  353.0 5.0 fusion.62
  358.1 1.2 constant_dynamic-slice_fusion.3
  359.3 2.8 fusion.64
  362.1 1.9 copy.24
  364.0 1.9 broadcast_divide_fusion
  366.8 9.9 %all-gather.27.cloned.1.call-done = bf16[2048,1024]{1,0:T(8,128)(2,1)} async-done(((bf16[128,1024]{1,0:T(8,128)(2,1)}), bf16[2048,1024]{1,0:T(8,128)(2,1)}) %all-gather.27.cloned.1.call-update) | async-done | bytes 4194320 | tf_op jit(solution)/shard_map/all_gather | solution.py:121
  376.7 5.9 fusion.34
  382.6 71.1 %all-gather.29.cloned.1.call-done = bf16[2048,1024]{1,0:T(8,128)(2,1)} async-done(((bf16[128,1024]{1,0:T(8,128)(2,1)}), bf16[2048,1024]{1,0:T(8,128)(2,1)}) %all-gather.29.cloned.1.call-update) | async-done | bytes 4194320 | tf_op jit(solution)/shard_map/all_gather | solution.py:122
  453.6 5.2 multiply_convert_fusion
  458.9 1.0 copy-done.3
  459.9 3.1 collective-permute-start
  463.0 2.4 collective-permute-start.1
  465.4 65.3 %all-gather.25.cloned.1.call-done = bf16[2048,1024]{1,0:T(8,128)(2,1)} async-done(((bf16[128,1024]{1,0:T(8,128)(2,1)}), bf16[2048,1024]{1,0:T(8,128)(2,1)}) %all-gather.25.cloned.1.call-update) | async-done | bytes 4194320 | tf_op jit(solution)/shard_map/all_gather | solution.py:120
  530.7 5.7 convolution_convert_fusion
  536.9 70.6 %all-gather.31.cloned.1.call-done = bf16[2048,1024]{1,0:T(8,128)(2,1)} async-done(((bf16[128,1024]{1,0:T(8,128)(2,1)}), bf16[2048,1024]{1,0:T(8,128)(2,1)}) %all-gather.31.cloned.1.call-update) | async-done | bytes 4194320 | tf_op jit(solution)/shard_map/all_gather | solution.py:124
  607.5 7.1 %fusion.24 = f32[512,2048]{1,0:T(8,128)} fusion(bf16[2048,1024]{1,0:T(8,128)(2,1)} %all-gather.31.cloned.1.call-done, f32[514,1024]{1,0:T(8,128)S(1)} %convert_element_type.49, bf16[512,1024]{1,0:T(8,128)(2,1)} %convolution_convert_fusion, f32[1024]{0:T(1024)S(1)} %bitcast.100, f32[1024]{0:T(1024)S(1)} %bitcast.99, f32[1024]{0:T(1024)S(1)} %bitcast.98), kind=kOutput, calls=%fused_computation.39 | convolution fusion | flops 2151677952 | bytes 15740928 | tf_op jit(solution)/shard_map/dot_general | solution.py:145
  614.6 54.9 %all-gather.23.cloned.1.call-done = bf16[2048,512]{1,0:T(8,128)(2,1)} async-done(((bf16[128,512]{1,0:T(8,128)(2,1)}), bf16[2048,512]{1,0:T(8,128)(2,1)}) %all-gather.23.cloned.1.call-update) | async-done | bytes 2097168 | tf_op jit(solution)/shard_map/all_gather | solution.py:123
  669.5 5.5 add_convert_fusion
  675.0 10.4 %reduce-scatter.2.cloned.1.call-done = bf16[256,2048]{1,0:T(8,128)(2,1)} async-done(((bf16[512,2048]{1,0:T(8,128)(2,1)}), bf16[256,2048]{1,0:T(8,128)(2,1)}) %reduce-scatter.2.cloned.1.call-update) | async-done | bytes 1048592 | tf_op jit(solution)/shard_map/reduce_scatter | solution.py:140
  (78 shorter events, 9.3 us)
Async XLA Ops:
  6.5 77.5 %copy-start.7 = (f32[2048]{0:T(1024)S(1)}, f32[2048]{0:T(1024)}, u32[]{:S(2)}) copy-start(f32[2048]{0:T(1024)} %param.18) | copy-start | bytes 24580
  6.5 14.8 %all-gather.33.cloned.1.call-start = ((), (), s32[]{:S(2)}) async-start(), calls=%async_computation.12 | async-start | bytes 3145728 | tf_op jit(solution)/shard_map/all_gather | solution.py:109
  7.3 76.8 %all-gather.13.cloned.1.call-start = ((), (), s32[]{:S(2)}) async-start(), calls=%async_computation.1 | async-start | bytes 2228224 | tf_op jit(solution)/shard_map/all_gather | solution.py:118
  8.0 138.0 %all-gather.19.cloned.1.call-start = ((), (), s32[]{:S(2)}) async-start(), calls=%async_computation.4 | async-start | bytes 2228224 | tf_op jit(solution)/shard_map/all_gather | solution.py:119
  8.7 199.1 %all-gather.17.cloned.1.call-start = ((), (), s32[]{:S(2)}) async-start(), calls=%async_computation.3 | async-start | bytes 2228224 | tf_op jit(solution)/shard_map/all_gather | solution.py:117
  9.3 243.6 %all-gather.15.cloned.1.call-start = ((), (), s32[]{:S(2)}) async-start(), calls=%async_computation.2 | async-start | bytes 2621440 | tf_op jit(solution)/shard_map/all_gather | solution.py:55
  21.4 62.7 %copy-start.1 = (bf16[1,512,2048]{2,1,0:T(8,128)(2,1)S(1)}, bf16[1,512,2048]{2,1,0:T(8,128)(2,1)}, u32[]{:S(2)}) copy-start(bf16[1,512,2048]{2,1,0:T(8,128)(2,1)} %all-gather.33.cloned.1.call-done) | copy-start | bytes 6291460
  88.0 65.5 %copy-start.8 = (f32[8]{0:T(128)S(1)}, f32[8]{0:T(128)}, u32[]{:S(2)}) copy-start(f32[8]{0:T(128)} %param.24) | copy-start | bytes 100
  88.0 210.8 %all-gather.21.cloned.1.call-start = ((), (), s32[]{:S(2)}) async-start(), calls=%async_computation.5 | async-start | bytes 2621440 | tf_op jit(solution)/shard_map/all_gather | solution.py:56
  149.7 226.9 %all-gather.27.cloned.1.call-start = ((), (), s32[]{:S(2)}) async-start(), calls=%async_computation.8 | async-start | bytes 4456448 | tf_op jit(solution)/shard_map/all_gather | solution.py:121
  150.5 303.2 %all-gather.29.cloned.1.call-start = ((), (), s32[]{:S(2)}) async-start(), calls=%async_computation.9 | async-start | bytes 4456448 | tf_op jit(solution)/shard_map/all_gather | solution.py:122
  151.2 379.4 %all-gather.25.cloned.1.call-start = ((), (), s32[]{:S(2)}) async-start(), calls=%async_computation.7 | async-start | bytes 4456448 | tf_op jit(solution)/shard_map/all_gather | solution.py:120
  152.0 455.5 %all-gather.31.cloned.1.call-start = ((), (), s32[]{:S(2)}) async-start(), calls=%async_computation.10 | async-start | bytes 4456448 | tf_op jit(solution)/shard_map/all_gather | solution.py:124
  152.6 516.9 %all-gather.23.cloned.1.call-start = ((), (), s32[]{:S(2)}) async-start(), calls=%async_computation.6 | async-start | bytes 2228224 | tf_op jit(solution)/shard_map/all_gather | solution.py:123
  153.3 532.1 %reduce-scatter.2.cloned.1.call-start = ((), (), s32[]{:S(2)}) async-start(), calls=%async_computation.11 | async-start | bytes 3145728 | tf_op jit(solution)/shard_map/reduce_scatter | solution.py:140
  154.6 57.0 %copy-start.5 = (f32[64]{0:T(128)S(1)}, f32[64]{0:T(128)}, u32[]{:S(2)}) copy-start(f32[64]{0:T(128)} %param.22) | copy-start | bytes 772
  308.5 6.4 copy-start
  323.4 6.3 copy-start
  338.2 6.3 copy-start
  353.0 6.3 copy-start
  365.9 0.7 copy-start.6
  365.9 10.8 %copy-start.2 = (bf16[1,512,2048]{2,1,0:T(8,128)(2,1)S(1)}, bf16[1,512,2048]{2,1,0:T(8,128)(2,1)}, u32[]{:S(2)}) copy-start(bf16[1,512,2048]{2,1,0:T(8,128)(2,1)} %all-gather.33.cloned.1.call-done) | copy-start | bytes 6291460
  458.9 1.0 copy-start.3
  459.9 76.5 %collective-permute-start = (bf16[1,1024]{1,0:T(2,128)(2,1)S(1)}, bf16[1,1024]{1,0:T(2,128)(2,1)S(1)}, u32[]{:S(2)}, u32[]{:S(2)}) collective-permute-start(bf16[1,1024]{1,0:T(2,128)(2,1)S(1)} %get-tuple-element.101), channel_id=1, source_target_pairs={{0,8},{8,16},{16,24},{1,9},{9,17},{17,25},{2,10},{10,18},{18,26},{... | collective-permute-start | bytes 6152 | tf_op jit(solution)/shard_map/ppermute | solution.py:18
  463.0 73.4 %collective-permute-start.1 = (bf16[1,1024]{1,0:T(2,128)(2,1)S(1)}, bf16[1,1024]{1,0:T(2,128)(2,1)S(1)}, u32[]{:S(2)}, u32[]{:S(2)}) collective-permute-start(bf16[1,1024]{1,0:T(2,128)(2,1)S(1)} %get-tuple-element.102), channel_id=1, source_target_pairs={{8,0},{16,8},{24,16},{9,1},{17,9},{25,17},{10,2},{18,10},{26,18},{... | collective-permute-start | bytes 6152 | tf_op jit(solution)/shard_map/ppermute | solution.py:19
  530.6 5.7 copy-start.4
Sparse Core Ops, SparseCore 0:
  8.9 12.4 all-gather.32
  24.1 59.8 all-gather.12
  86.8 59.1 all-gather.18
  148.6 59.1 all-gather.16
  209.3 43.5 all-gather.14
  254.3 44.4 all-gather.20
  301.6 75.0 all-gather.26
  379.4 74.1 all-gather.28
  456.4 74.1 all-gather.24
  533.3 74.1 all-gather.30
  610.3 59.1 all-gather.22
  675.2 10.1 reduce-scatter.1
where the time goes:
time: 694 us; the launch traced here: 692 us
  waiting for transfers between devices  550 us (79%)
  matrix products  73.5 us (11%)
  other arithmetic  26.7 us (4%)
  local copies, waits for them, and re-layouts  21.7 us (3%)
  between operations  13.8 us (2%)
    all_gather x1, waiting for transfers between devices, per_device(): lax.all_gather(inner_weight, ('sp', 'fs'), axis=0, tiled=True)  71.1 us
    all_gather x1, waiting for transfers between devices, per_device(): lax.all_gather(conv_out_weight, ('sp', 'fs'), axis=0, tiled=True)  70.6 us
    all_gather x1, waiting for transfers between devices, per_device(): lax.all_gather(post_gate_weight, ('sp', 'fs'), axis=0, tiled=True)  65.3 us
    all_gather x1, waiting for transfers between devices, per_device(): lax.all_gather(key_weight, ('sp', 'fs'), axis=0, tiled=True)  60.4 us
    all_gather x1, waiting for transfers between devices, per_device(): lax.all_gather(value_weight, ('sp', 'fs'), axis=0, tiled=True)  57.9 us
    all_gather x1, waiting for transfers between devices, per_device(): lax.all_gather(attn_out_weight, ('sp', 'fs'), axis=0, tiled=True)  54.9 us
    all_gather x1, waiting for transfers between devices, per_device(): lax.all_gather(query_weight, ('sp', 'fs'), axis=0, tiled=True)  53.3 us
    all_gather x1, waiting for transfers between devices, attention_branch(): key_piece = lax.all_gather(key_normed, 'sp', axis=0, tiled=True)  41.2 us
  transfers between devices with their start and end apart: 14, of which 12 were waited for; matrix products, arithmetic and copies ran while one was open for 17% of the time, Pallas kernels for 0%

commit v1 on v0

--- a/solution.py
+++ b/solution.py
@@ -3,6 +3,8 @@
 import jax
 import jax.numpy as jnp
 from jax import lax
+from jax.experimental import pallas as pl
+from jax.experimental.pallas import tpu as pltpu
 from jax.sharding import PartitionSpec as P
 
 epsilon = 1e-06
@@ -86,6 +88,149 @@
     head_out = mapped[:, 0] - weight_two[:, None, None] * mapped[:, 1]
     normed_out = scale_rows(head_out, head_gain).astype(jnp.bfloat16)
     return jnp.transpose(normed_out, (1, 0, 2)).reshape(tok_rows, heads * vsize)
+
+
+def half_scaled(values, gain, half):
+    low = lax.broadcasted_iota(jnp.int32, (1, 2 * half), 1) < half
+    squares = values * values
+    first = jnp.sum(jnp.where(low, squares, 0.0), axis=-1, keepdims=True) / half
+    second = jnp.sum(jnp.where(low, 0.0, squares), axis=-1, keepdims=True) / half
+    factor = jnp.where(low, lax.rsqrt(first + epsilon), lax.rsqrt(second + epsilon))
+    return values * factor * gain
+
+
+def attention_kernel(half, q_ref, k_ref, v_ref, qg_ref, kg_ref, lam_ref, hg_ref, out_ref, key, val):
+    @pl.when(pl.program_id(1) == 0)
+    def _():
+        key[...] = half_scaled(k_ref[...], kg_ref[...], half).astype(jnp.bfloat16)
+        val[...] = v_ref[...].astype(jnp.bfloat16)
+
+    low = lax.broadcasted_iota(jnp.int32, (1, 2 * half), 1) < half
+    query = half_scaled(q_ref[...], qg_ref[...], half).astype(jnp.bfloat16).astype(jnp.float32)
+    maps = []
+    for which in range(2):
+        keep = low if which == 0 else jnp.logical_not(low)
+        part = jnp.where(keep, query, 0.0).astype(jnp.bfloat16)
+        scores = lax.dot_general(
+            part, key[...], (((1,), (1,)), ((), ())), preferred_element_type=jnp.float32
+        ) * half ** (-0.5)
+        expo = jnp.exp(scores - jnp.max(scores, axis=-1, keepdims=True))
+        total = jnp.sum(expo, axis=-1, keepdims=True)
+        maps.append(
+            jnp.dot(expo.astype(jnp.bfloat16), val[...], preferred_element_type=jnp.float32) / total
+        )
+    head_out = maps[0] - lam_ref[0] * maps[1]
+    out_ref[...] = scale_rows(head_out, hg_ref[...]).astype(jnp.bfloat16)
+
+
+def attention_call(y, heads, query_gain, key_gain, weight_two, head_gain):
+    rows = y.shape[0]
+    half, vsize = query_gain.shape[0], head_gain.shape[0]
+    block = math.gcd(rows, 256)
+    small = lambda h, i: (0, 0)
+    return pl.pallas_call(
+        lambda *refs: attention_kernel(half, *refs),
+        out_shape=jax.ShapeDtypeStruct((rows, heads * vsize), jnp.bfloat16),
+        grid=(heads, rows // block),
+        in_specs=[
+            pl.BlockSpec((block, 2 * half), lambda h, i: (i, h)),
+            pl.BlockSpec((rows, 2 * half), lambda h, i: (0, heads + h)),
+            pl.BlockSpec((rows, vsize), lambda h, i: (0, 2 * heads + h)),
+            pl.BlockSpec((1, 2 * half), small),
+            pl.BlockSpec((1, 2 * half), small),
+            pl.BlockSpec((1, 1, vsize), lambda h, i: (h, 0, 0)),
+            pl.BlockSpec((1, vsize), small),
+        ],
+        out_specs=pl.BlockSpec((block, vsize), lambda h, i: (i, h)),
+        scratch_shapes=[
+            pltpu.VMEM((rows, 2 * half), jnp.bfloat16),
+            pltpu.VMEM((rows, vsize), jnp.bfloat16),
+        ],
+        compiler_params=pltpu.CompilerParams(vmem_limit_bytes=40 * 2**20),
+        cost_estimate=pl.CostEstimate(
+            flops=heads * rows * rows * 8 * half * 2,
+            bytes_accessed=rows * heads * vsize * 14,
+            transcendentals=2 * heads * rows * rows,
+        ),
+    )(
+        y,
+        y,
+        y,
+        jnp.tile(query_gain, 2)[None],
+        jnp.tile(key_gain, 2)[None],
+        jnp.broadcast_to(weight_two[:, None, None], (heads, 1, vsize)),
+        head_gain[None],
+    )
+
+
+def column_parts(weights, parts):
+    rows = weights[0].shape[0]
+    pieces = [w.reshape(rows, parts, w.shape[1] // parts) for w in weights]
+    return jnp.transpose(jnp.concatenate(pieces, axis=2), (1, 0, 2))
+
+
+def gathered_rows(packed):
+    mine = lax.all_to_all(packed, "sp", split_axis=0, concat_axis=0, tiled=True)
+    every = lax.all_gather(mine, "fs", axis=1, tiled=False)
+    return every.reshape(-1, packed.shape[2])
+
+
+def split_device(
+    inputs,
+    norm_gain,
+    query_weight,
+    key_weight,
+    value_weight,
+    query_gain,
+    key_gain,
+    mix_lambda,
+    head_gain,
+    post_gate_weight,
+    pre_gate_weight,
+    inner_weight,
+    conv_taps,
+    attn_out_weight,
+    conv_out_weight,
+):
+    sp, tp = lax.axis_size("sp"), lax.axis_size("tp")
+    tokens = inputs[0]
+    place = lax.axis_index("tp") * sp + lax.axis_index("sp")
+    vsize = head_gain.shape[0]
+    heads = value_weight.shape[1] // vsize // sp
+    channels = post_gate_weight.shape[1] // sp
+    weight_two = lax.dynamic_slice_in_dim(mix_lambda, place * heads, heads)
+    taps = lax.dynamic_slice_in_dim(conv_taps, place * channels, channels, 1)
+    into = gathered_rows(
+        column_parts(
+            (query_weight, key_weight, value_weight, post_gate_weight, pre_gate_weight, inner_weight),
+            sp,
+        )
+    )
+    outof = gathered_rows(column_parts((attn_out_weight, conv_out_weight), sp))
+    along = lax.all_gather(tokens, "sp", axis=0, tiled=True)
+    both = lax.all_gather(along, "tp", axis=0, tiled=False)
+    whole = jnp.concatenate([both[i] for i in range(tp)], axis=1)
+    normed = scale_rows(whole.astype(jnp.float32), norm_gain).astype(jnp.bfloat16)
+    y = jnp.dot(normed, into, preferred_element_type=jnp.float32)
+    attn_hidden = attention_call(y, heads, query_gain, key_gain, weight_two, head_gain)
+    span = 3 * heads * vsize
+    post, pre_gate, inner = [
+        y[:, span + i * channels : span + (i + 1) * channels] for i in range(3)
+    ]
+    post_wide = lax.optimization_barrier(post.astype(jnp.bfloat16)).astype(jnp.float32)
+    signal = lax.optimization_barrier((pre_gate * inner).astype(jnp.bfloat16))
+    shifted = jnp.pad(signal.astype(jnp.float32), ((1, 1), (0, 0)))
+    filtered = taps[0] * shifted[:-2] + taps[1] * shifted[1:-1] + taps[2] * shifted[2:]
+    conv_hidden = (post_wide * filtered).astype(jnp.bfloat16)
+    hidden = jnp.concatenate([attn_hidden, conv_hidden], axis=1)
+    width = hidden.shape[1]
+    hidden = hidden.reshape(sp, tp, -1, width).transpose(1, 0, 2, 3).reshape(-1, width)
+    partial = lax.dot_general(
+        hidden, outof, (((1,), (1,)), ((), ())), preferred_element_type=jnp.float32
+    ).astype(jnp.bfloat16)
+    summed = lax.psum_scatter(partial, "tp", scatter_dimension=0, tiled=True)
+    summed = lax.psum_scatter(summed, "sp", scatter_dimension=0, tiled=True)
+    return summed[None]
 
 
 def per_device(
@@ -171,10 +316,20 @@
         P(("sp", "fs"), "tp"),
         P(("sp", "fs"), "tp"),
     )
-    return jax.shard_map(
-        per_device,
+    sp, tp = mesh.shape["sp"], mesh.shape["tp"]
+
+    def program(*args):
+        heads = args[7].shape[0]
+        channels = args[12].shape[1]
+        splits = heads % (sp * tp) == 0 and channels % (sp * tp * 128) == 0
+        return shard(split_device if splits else per_device)(*args)
+
+    shard = lambda body: jax.shard_map(
+        body,
         mesh=mesh,
         in_specs=placed,
         out_specs=P("fs", ("sp", "tp"), None),
         check_vma=False,
     )
+
+    return program

time: 694 us -> 385 us (0.55)
  waiting for transfers between devices: 550 us -> 243 us
  blocking collectives: 0 us -> 59.2 us
  matrix products: 73.5 us -> 20.4 us
  other arithmetic: 26.7 us -> 4.1 us
  Pallas kernels: 0 us -> 18.2 us
    all_gather x11 -> x4, waiting for transfers between devices: 534 us -> 133 us  [the longest x2 88.8 us: gathered_rows(): every = lax.all_gather(mine, 'fs', axis=1, tiled=False)]
    reduce_scatter x1 -> x2, waiting for transfers between devices: 10.4 us -> 97.1 us  [the longest x1 79.5 us: split_device(): summed = lax.psum_scatter(summed, 'sp', scatter_dimension=0, tiled=True)]
    all_to_all x0 -> x1, blocking collectives: none -> 59.2 us  [gathered_rows(): mine = lax.all_to_all(packed, 'sp', split_axis=0, concat_axis=0, tiled=True)]
    dot_general x16 -> x2, matrix products: 73.5 us -> 20.4 us  [the longest x1 13.5 us: split_device(): y = jnp.dot(normed, into, preferred_element_type=jnp.float32)]
    reduce_sum x4 -> x0, other arithmetic: 20.1 us -> none  [one_block(): total = total * factor + jnp.sum(expo, axis=-1)]
    pallas_call x0 -> x1, Pallas kernels: none -> 18.2 us  [attention_call(): pl.pallas_call(lambda *refs: attention_kernel(half, *refs), out_shape=jax...]
    all_to_all x0 -> x1, waiting for transfers between devices: none -> 12.2 us  [gathered_rows(): mine = lax.all_to_all(packed, 'sp', split_axis=0, concat_axis=0, tiled=True)]
    all_gather x0 -> x2, local copies, waits for them, and re-layouts: none -> 8.58 us  [gathered_rows(): every = lax.all_gather(mine, 'fs', axis=1, tiled=False)]
  transfers between devices with their start and end apart: 14 -> 7, of which waited for: 12 -> 7; matrix products, arithmetic and copies ran while one was open for 17% -> 4% of each run, Pallas kernels for 0% -> 0%
where the time goes in v1:
time: 385 us; the launch traced here: 383 us
  waiting for transfers between devices  243 us (63%)
  blocking collectives  59.2 us (15%)
  matrix products  20.4 us (5%)
  local copies, waits for them, and re-layouts  19.6 us (5%)
  Pallas kernels  18.2 us (5%)
  between operations  13.8 us (4%)
  starting transfers between devices  4.92 us (1%)
  other arithmetic  4.1 us (1%)
    all_gather x2, waiting for transfers between devices, gathered_rows(): every = lax.all_gather(mine, 'fs', axis=1, tiled=False)  88.8 us
    reduce_scatter x1, waiting for transfers between devices, split_device(): summed = lax.psum_scatter(summed, 'sp', scatter_dimension=0, tiled=True)  79.5 us
    all_to_all x1, blocking collectives, gathered_rows(): mine = lax.all_to_all(packed, 'sp', split_axis=0, concat_axis=0, tiled=True)  59.2 us
    all_gather x1, waiting for transfers between devices, split_device(): along = lax.all_gather(tokens, 'sp', axis=0, tiled=True)  28.5 us
    pallas_call x1, Pallas kernels, attention_call(): pl.pallas_call(lambda *refs: attention_kernel(half, *refs), out_shape=jax...  18.2 us
    reduce_scatter x1, waiting for transfers between devices, split_device(): summed = lax.psum_scatter(partial, 'tp', scatter_dimension=0, tiled=True)  17.7 us
    all_gather x1, waiting for transfers between devices, split_device(): both = lax.all_gather(along, 'tp', axis=0, tiled=False)  15.5 us
    dot_general x1, matrix products, split_device(): y = jnp.dot(normed, into, preferred_element_type=jnp.float32)  13.5 us
  transfers between devices with their start and end apart: 7, of which 7 were waited for; matrix products, arithmetic and copies ran while one was open for 4% of the time, Pallas kernels for 0%

profile of v1, /device:TPU:9, one launch (start us, length us, event | category | flops | bytes accessed | tf_op | source)
XLA Modules:
  0.0 383.1 jit_solution(15021679303804144606)
XLA Ops:
  6.5 0.7 all-gather.9.cloned.1.call-update
  7.3 1.2 copy.37
  8.5 1.0 copy.36
  9.5 0.8 maximum_bitcast_fusion
  10.3 4.8 %all-to-all-start.1 = ((bf16[4,128,384]{1,2,0:T(8,128)(2,1)}), bf16[4,128,384]{1,2,0:T(8,128)(2,1)S(1)}, u32[]{:S(2)}, u32[]{:S(2)}) async-start(bf16[4,128,384]{1,2,0:T(8,128)(2,1)} %maximum_bitcast_fusion), calls=%async_computation.1 | async-start | bytes 786432 | tf_op jit(solution)/shard_map/all_to_all | solution.py:173
  15.0 0.1 copy.28
  15.2 12.2 %all-to-all-done.1 = bf16[4,128,384]{1,2,0:T(8,128)(2,1)S(1)} async-done(((bf16[4,128,384]{1,2,0:T(8,128)(2,1)}), bf16[4,128,384]{1,2,0:T(8,128)(2,1)S(1)}, u32[]{:S(2)}, u32[]{:S(2)}) %all-to-all-start.1) | async-done | bytes 393248 | tf_op jit(solution)/shard_map/all_to_all | solution.py:173
  27.4 0.7 copy-done.1
  28.1 0.0 all-gather.15.cloned.1.call-update
  28.2 0.0 all-gather.13.cloned.1.call-start
  28.2 0.1 copy.29
  28.4 0.1 copy.30
  28.5 0.2 copy.31
  28.7 0.2 copy.32
  28.9 0.2 copy.33
  29.2 59.2 %all_to_all.10 = bf16[4,128,1152]{1,2,0:T(8,128)(2,1)} all-to-all(bf16[4,128,1152]{1,2,0:T(8,128)(2,1)S(1)} %bitcast.35), channel_id=1, replica_groups=mesh['sp'=4,'fs'=4,'tp'=2] {'sp'}, dimensions={0} | all-to-all | bytes 2359296 | tf_op jit(solution)/shard_map/all_to_all | solution.py:173
  88.4 0.0 all-gather.13.cloned.1.call-update
  88.4 0.0 all-gather.11.cloned.1.call-start
  88.5 28.5 %all-gather.9.cloned.1.call-done = bf16[1,2048,1024]{2,1,0:T(8,128)(2,1)} async-done(((bf16[1,512,1024]{2,1,0:T(8,128)(2,1)}), bf16[1,2048,1024]{2,1,0:T(8,128)(2,1)}) %all-gather.9.cloned.1.call-update) | async-done | bytes 4194320 | tf_op jit(solution)/shard_map/all_gather | solution.py:210
  117.0 0.0 all-gather.11.cloned.1.call-update
  117.0 0.0 reduce-scatter.3.cloned.1.call-start
  117.1 0.6 copy-done.9
  117.7 0.1 broadcast_in_dim_tile.6.refs_3_
  117.7 0.1 broadcast_in_dim_tile.7.refs_4_
  117.8 0.6 dynamic_slice.6
  118.4 0.9 constant_dynamic-slice_fusion
  119.3 32.0 %all-gather.15.cloned.1.call-done = bf16[4,512,384]{1,2,0:T(8,128)(2,1)} async-done(((bf16[4,128,384]{1,2,0:T(8,128)(2,1)}), bf16[4,512,384]{1,2,0:T(8,128)(2,1)}) %all-gather.15.cloned.1.call-update) | async-done | bytes 1572880 | tf_op jit(solution)/shard_map/all_gather | solution.py:174
  151.3 1.9 copy.38
  153.2 56.8 %all-gather.13.cloned.1.call-done = bf16[4,512,1152]{1,2,0:T(8,128)(2,1)} async-done(((bf16[4,128,1152]{1,2,0:T(8,128)(2,1)}), bf16[4,512,1152]{1,2,0:T(8,128)(2,1)}) %all-gather.13.cloned.1.call-update) | async-done | bytes 4718608 | tf_op jit(solution)/shard_map/all_gather | solution.py:174
  210.0 6.7 %copy.34 = bf16[4,512,1152]{2,1,0:T(8,128)(2,1)} copy(bf16[4,512,1152]{1,2,0:T(8,128)(2,1)} %all-gather.13.cloned.1.call-done) | data formatting | bytes 9437184 | tf_op jit(solution)/shard_map/all_gather | solution.py:174
  216.7 15.5 %all-gather.11.cloned.1.call-done = bf16[2,2048,1024]{2,1,0:T(8,128)(2,1)} async-done(((bf16[1,2048,1024]{2,1,0:T(8,128)(2,1)}), bf16[2,2048,1024]{2,1,0:T(8,128)(2,1)}) %all-gather.11.cloned.1.call-update) | async-done | bytes 8388624 | tf_op jit(solution)/shard_map/all_gather | solution.py:211
  232.2 4.0 %slice_bitcast_fusion.1 = (bf16[2048,1024]{1,0:T(8,128)(2,1)S(1)}, bf16[2048,1024]{1,0:T(8,128)(2,1)S(1)}) fusion(bf16[2,2048,1024]{2,1,0:T(8,128)(2,1)} %all-gather.11.cloned.1.call-done), kind=kLoop, calls=%fused_computation.11 | loop fusion | bytes 16777216 | tf_op jit(solution)/shard_map/squeeze | solution.py:212
  236.2 1.9 fusion
  238.1 13.5 %fusion.3.refs_0_.refs_1_.refs_2_ = f32[2048,1152]{1,0:T(8,128)S(1)} fusion(bf16[2048,1152]{1,0:T(8,128)(2,1)} %bitcast.32, f32[2048]{0:T(1024)S(1)} %copy-done.8, f32[2048]{0:T(1024)S(1)} %add_rsqrt_fusion, bf16[2048,1024]{1,0:T(8,128)(2,1)S(1)} %get-tuple-element.6, bf16[2048,1024]{1,0:T(8,128)(2,1)S(1)} %get-tuple-element.5), kind=kOutput, calls=%fused_computation.5 | convolution fusion | flops 9693036544 | bytes 22560768 | tf_op jit(solution)/shard_map/dot_general | solution.py:214
  251.6 0.2 fusion.7
  251.8 0.1 slice.56
  252.0 0.2 convert_element_type.28
  252.1 0.6 broadcast_in_dim.17.refs_5_
  252.7 18.2 %shard_map.145 = bf16[2048,128]{1,0:T(8,128)(2,1)S(1)} custom-call(f32[2048,1152]{1,0:T(8,128)S(1)} %fusion.3.refs_0_.refs_1_.refs_2_, f32[2048,1152]{1,0:T(8,128)S(1)} %fusion.3.refs_0_.refs_1_.refs_2_, f32[2048,1152]{1,0:T(8,128)S(1)} %fusion.3.refs_0_.refs_1_.refs_2_, f32[1,128]{1,0:T(1,128)S(1)} %broadcast_in_dim_tile.6.refs_3_, ...), custom_call_target="tpu_custom_call" | custom-call | flops 4294967296 | bytes 3670016 | tf_op jit(solution)/shard_map/pallas_call | solution.py:131
  270.9 0.8 multiply_convert_fusion
  271.8 0.2 pad_maximum_fusion.2
  272.0 0.2 copy.35
  272.1 6.9 %convolution_convert_fusion = bf16[2048,2048]{1,0:T(8,128)(2,1)} fusion(bf16[2048,384]{1,0:T(8,128)(2,1)S(1)} %bitcast.34, bf16[2048,384]{1,0:T(8,128)(2,1)S(1)} %bitcast.33), kind=kOutput, calls=%fused_computation.9 | convolution fusion | flops 3225419776 | bytes 11534336 | tf_op jit(solution)/shard_map/dot_general | solution.py:228
  279.1 0.0 reduce-scatter.3.cloned.1.call-update
  279.1 0.0 reduce-scatter.5.cloned.1.call-start
  279.1 17.7 %reduce-scatter.3.cloned.1.call-done = bf16[1024,2048]{1,0:T(8,128)(2,1)} async-done(((bf16[2048,2048]{1,0:T(8,128)(2,1)}), bf16[1024,2048]{1,0:T(8,128)(2,1)}) %reduce-scatter.3.cloned.1.call-update) | async-done | bytes 4194320 | tf_op jit(solution)/shard_map/reduce_scatter | solution.py:231
  296.8 0.0 reduce-scatter.5.cloned.1.call-update
  296.8 79.5 %reduce-scatter.5.cloned.1.call-done = bf16[256,2048]{1,0:T(8,128)(2,1)} async-done(((bf16[1024,2048]{1,0:T(8,128)(2,1)}), bf16[256,2048]{1,0:T(8,128)(2,1)}) %reduce-scatter.5.cloned.1.call-update) | async-done | bytes 1048592 | tf_op jit(solution)/shard_map/reduce_scatter | solution.py:232
  (33 shorter events, 0.2 us)
Async XLA Ops:
  6.5 8.5 %copy-start.5 = (bf16[128,512]{1,0:T(8,128)(2,1)S(1)}, bf16[128,512]{1,0:T(8,128)(2,1)}, u32[]{:S(2)}) copy-start(bf16[128,512]{1,0:T(8,128)(2,1)} %param.17) | copy-start | bytes 393220
  6.5 21.7 %copy-start.6 = (bf16[128,512]{1,0:T(8,128)(2,1)S(1)}, bf16[128,512]{1,0:T(8,128)(2,1)}, u32[]{:S(2)}) copy-start(bf16[128,512]{1,0:T(8,128)(2,1)} %param.18) | copy-start | bytes 393220
  6.5 21.8 %copy-start.7 = (bf16[128,512]{1,0:T(8,128)(2,1)S(1)}, bf16[128,512]{1,0:T(8,128)(2,1)}, u32[]{:S(2)}) copy-start(bf16[128,512]{1,0:T(8,128)(2,1)} %param.19) | copy-start | bytes 393220
  6.5 110.5 %all-gather.9.cloned.1.call-start = ((), (), s32[]{:S(2)}) async-start(), calls=%async_computation.6 | async-start | bytes 5242880 | tf_op jit(solution)/shard_map/all_gather | solution.py:210
  7.3 21.2 %copy-start.2 = (bf16[128,1024]{1,0:T(8,128)(2,1)S(1)}, bf16[128,1024]{1,0:T(8,128)(2,1)}, u32[]{:S(2)}) copy-start(bf16[128,1024]{1,0:T(8,128)(2,1)} %param.24) | copy-start | bytes 786436
  7.3 21.4 %copy-start.3 = (bf16[128,1024]{1,0:T(8,128)(2,1)S(1)}, bf16[128,1024]{1,0:T(8,128)(2,1)}, u32[]{:S(2)}) copy-start(bf16[128,1024]{1,0:T(8,128)(2,1)} %param.25) | copy-start | bytes 786436
  9.5 19.4 %copy-start.4 = (bf16[128,1024]{1,0:T(8,128)(2,1)S(1)}, bf16[128,1024]{1,0:T(8,128)(2,1)}, u32[]{:S(2)}) copy-start(bf16[128,1024]{1,0:T(8,128)(2,1)} %param.26) | copy-start | bytes 786436
  10.3 17.1 %all-to-all-start.1 = ((bf16[4,128,384]{1,2,0:T(8,128)(2,1)}), bf16[4,128,384]{1,2,0:T(8,128)(2,1)S(1)}, u32[]{:S(2)}, u32[]{:S(2)}) async-start(bf16[4,128,384]{1,2,0:T(8,128)(2,1)} %maximum_bitcast_fusion), calls=%async_computation.1 | async-start | bytes 786432 | tf_op jit(solution)/shard_map/all_to_all | solution.py:173
  15.0 136.3 %all-gather.15.cloned.1.call-start = ((), (), s32[]{:S(2)}) async-start(), calls=%async_computation.9 | async-start | bytes 1966080 | tf_op jit(solution)/shard_map/all_gather | solution.py:174
  27.4 0.7 copy-start.1
  28.2 181.8 %all-gather.13.cloned.1.call-start = ((), (), s32[]{:S(2)}) async-start(), calls=%async_computation.8 | async-start | bytes 5898240 | tf_op jit(solution)/shard_map/all_gather | solution.py:174
  88.4 143.7 %all-gather.11.cloned.1.call-start = ((), (), s32[]{:S(2)}) async-start(), calls=%async_computation.7 | async-start | bytes 12582912 | tf_op jit(solution)/shard_map/all_gather | solution.py:211
  117.0 0.7 copy-start.9
  117.0 0.7 copy-start.10
  117.0 0.8 copy-start.11
  117.0 179.8 %reduce-scatter.3.cloned.1.call-start = ((), (), s32[]{:S(2)}) async-start(), calls=%async_computation.4 | async-start | bytes 12582912 | tf_op jit(solution)/shard_map/reduce_scatter | solution.py:231
  236.1 2.0 copy-start.8
  252.0 0.8 copy-start
  279.1 97.2 %reduce-scatter.5.cloned.1.call-start = ((), (), s32[]{:S(2)}) async-start(), calls=%async_computation.5 | async-start | bytes 5242880 | tf_op jit(solution)/shard_map/reduce_scatter | solution.py:232
Sparse Core Ops, SparseCore 0:
  8.9 108.0 all-gather.8
  118.8 32.4 all-gather.14
  153.1 56.7 all-gather.12
  211.4 20.7 all-gather.10
  279.2 17.5 reduce-scatter.2
  298.9 77.3 reduce-scatter.4

commit v2 on v1

--- a/solution.py
+++ b/solution.py
@@ -169,10 +169,191 @@
     return jnp.transpose(jnp.concatenate(pieces, axis=2), (1, 0, 2))
 
 
-def gathered_rows(packed):
-    mine = lax.all_to_all(packed, "sp", split_axis=0, concat_axis=0, tiled=True)
-    every = lax.all_gather(mine, "fs", axis=1, tiled=False)
-    return every.reshape(-1, packed.shape[2])
+def remote(source, target, send, recv, where):
+    return pltpu.make_async_remote_copy(
+        src_ref=source,
+        dst_ref=target,
+        send_sem=send,
+        recv_sem=recv,
+        device_id=where,
+        device_id_type=pl.DeviceIdType.MESH,
+    )
+
+
+def meet(places):
+    barrier = pltpu.get_barrier_semaphore()
+    for where in places:
+        pl.semaphore_signal(
+            barrier, inc=1, device_id=where, device_id_type=pl.DeviceIdType.MESH
+        )
+    pl.semaphore_wait(barrier, len(places))
+
+
+def gather_kernel(
+    n, w_ref, t_ref, w_all, t_all, own, z_send, z_recv, f_send, f_recv, g_send, g_recv,
+    t_send, t_recv, p_send, p_recv,
+):
+    z, f, c = lax.axis_index("sp"), lax.axis_index("fs"), lax.axis_index("tp")
+    beside, above = f + 1 - 2 * (f % 2), f + 2 - 4 * (f // 2)
+    rows = t_ref.shape[0]
+    near = sorted(range(1, n), key=lambda d: min(d, n - d))
+    meet(
+        [{"sp": (z + d) % n} for d in near] + [{"fs": beside}, {"fs": above}, {"tp": 1 - c}]
+    )
+
+    def place(s):
+        return t_all.at[c, pl.ds(pl.multiple_of(s * rows, rows), rows)]
+
+    flights = []
+
+    def go(copy):
+        copy.start()
+        flights.append(copy)
+        return copy
+
+    across = {
+        d: go(
+            remote(
+                w_ref.at[(z + d) % n], w_all.at[z, f], z_send.at[d], z_recv.at[d], {"sp": (z + d) % n}
+            )
+        )
+        for d in near
+    }
+    side = {}
+
+    def spread(d, source):
+        s = (z + n - d) % n
+        for i, to in enumerate((beside, above)):
+            side[i, d] = go(
+                remote(source, w_all.at[s, f], f_send.at[i, d], f_recv.at[i, d], {"fs": to})
+            )
+
+    def pass_on(d):
+        s = (z + n - d) % n
+        i = d % 2
+        side[i, d].wait_recv()
+        held, to = (beside, above) if i == 0 else (above, beside)
+        go(remote(w_all.at[s, held], w_all.at[s, held], g_send.at[d], g_recv.at[d], {"fs": to}))
+
+    spread(0, w_ref.at[z])
+    tokens = {
+        d: go(remote(t_ref, place(z), t_send.at[d], t_recv.at[d], {"sp": (z + d) % n}))
+        for d in near
+    }
+    go(remote(t_ref, place(z), p_send.at[0], p_recv.at[0], {"tp": 1 - c}))
+    mine = [
+        pltpu.make_async_copy(w_ref.at[z], w_all.at[z, f], own.at[0]),
+        pltpu.make_async_copy(t_ref, place(z), own.at[1]),
+    ]
+    for copy in mine:
+        copy.start()
+    last = 0
+    for d in near:
+        across[d].wait_recv()
+        spread(d, w_all.at[(z + n - d) % n, f])
+        pass_on(last)
+        last = d
+    pass_on(last)
+    for d in near:
+        tokens[d].wait_recv()
+        s = (z + n - d) % n
+        go(remote(place(s), place(s), p_send.at[d], p_recv.at[d], {"tp": 1 - c}))
+    waited = set(map(id, across.values())) | set(map(id, tokens.values()))
+    waited |= {id(side[d % 2, d]) for d in range(n)}
+    for copy in flights:
+        copy.wait_send()
+        if id(copy) not in waited:
+            copy.wait_recv()
+    for copy in mine:
+        copy.wait()
+
+
+def gather_all(packed, tokens):
+    n, rows, columns = packed.shape
+    fs, tp = lax.axis_size("fs"), lax.axis_size("tp")
+    dma = pltpu.SemaphoreType.DMA
+    return pl.pallas_call(
+        lambda *refs: gather_kernel(n, *refs),
+        out_shape=(
+            jax.ShapeDtypeStruct((n, fs, rows, columns), packed.dtype),
+            jax.ShapeDtypeStruct((tp, n * tokens.shape[0], tokens.shape[1]), tokens.dtype),
+        ),
+        in_specs=[pl.BlockSpec(memory_space=pltpu.VMEM)] * 2,
+        out_specs=(pl.BlockSpec(memory_space=pl.ANY),) * 2,
+        scratch_shapes=[
+            dma((2,)), dma((n,)), dma((n,)), dma((2, n)), dma((2, n)), dma((n,)), dma((n,)),
+            dma((n,)), dma((n,)), dma((n,)), dma((n,)),
+        ],
+        compiler_params=pltpu.CompilerParams(collective_id=1, has_side_effects=True),
+    )(packed, tokens)
+
+
+def reduce_kernel(n, p_ref, out_ref, twin, pair, others, a_send, a_recv, b_send, b_recv):
+    z, c = lax.axis_index("sp"), lax.axis_index("tp")
+    near = sorted(range(1, n), key=lambda d: -min(d, n - d))
+    meet([{"sp": (z + d) % n} for d in near] + [{"tp": 1 - c}])
+    rows = out_ref.shape[0]
+    tile = math.gcd(rows, 32)
+    swaps = {}
+    for d in near + [0]:
+        s = (z + d) % n
+        swaps[d] = remote(
+            p_ref.at[1 - c, s], twin.at[d], a_send.at[d], a_recv.at[d], {"tp": 1 - c}
+        )
+        swaps[d].start()
+    sends = {}
+    for d in near + [0]:
+        s = (z + d) % n
+        swaps[d].wait_recv()
+
+        def add(i, unused, s=s, d=d):
+            at = pl.ds(pl.multiple_of(i * tile, tile), tile)
+            total = p_ref[c, s, at, :].astype(jnp.float32) + twin[d, at, :].astype(jnp.float32)
+            pair[d, at, :] = total.astype(jnp.bfloat16)
+            return unused
+
+        lax.fori_loop(0, rows // tile, add, 0)
+        if d:
+            sends[d] = remote(
+                pair.at[d], others.at[d - 1], b_send.at[d - 1], b_recv.at[d - 1], {"sp": s}
+            )
+            sends[d].start()
+    for d in near:
+        sends[d].wait_recv()
+
+    def finish(i, unused):
+        at = pl.ds(pl.multiple_of(i * tile, tile), tile)
+        total = pair[0, at, :].astype(jnp.float32)
+        for d in range(1, n):
+            total += others[d - 1, at, :].astype(jnp.float32)
+        out_ref[at, :] = total.astype(jnp.bfloat16)
+        return unused
+
+    lax.fori_loop(0, rows // tile, finish, 0)
+    for d in near + [0]:
+        swaps[d].wait_send()
+    for d in near:
+        sends[d].wait_send()
+
+
+def reduce_all(partial):
+    tp, n, rows, width = partial.shape
+    dma = pltpu.SemaphoreType.DMA
+    return pl.pallas_call(
+        lambda *refs: reduce_kernel(n, *refs),
+        out_shape=jax.ShapeDtypeStruct((rows, width), partial.dtype),
+        in_specs=[pl.BlockSpec(memory_space=pltpu.VMEM)],
+        out_specs=pl.BlockSpec(memory_space=pltpu.VMEM),
+        scratch_shapes=[
+            pltpu.VMEM((n, rows, width), partial.dtype),
+            pltpu.VMEM((n, rows, width), partial.dtype),
+            pltpu.VMEM((n - 1, rows, width), partial.dtype),
+            dma((n,)), dma((n,)), dma((n - 1,)), dma((n - 1,)),
+        ],
+        compiler_params=pltpu.CompilerParams(
+            collective_id=2, has_side_effects=True, vmem_limit_bytes=48 * 2**20
+        ),
+    )(partial)
 
 
 def split_device(
@@ -200,15 +381,23 @@
     channels = post_gate_weight.shape[1] // sp
     weight_two = lax.dynamic_slice_in_dim(mix_lambda, place * heads, heads)
     taps = lax.dynamic_slice_in_dim(conv_taps, place * channels, channels, 1)
-    into = gathered_rows(
-        column_parts(
-            (query_weight, key_weight, value_weight, post_gate_weight, pre_gate_weight, inner_weight),
-            sp,
-        )
-    )
-    outof = gathered_rows(column_parts((attn_out_weight, conv_out_weight), sp))
-    along = lax.all_gather(tokens, "sp", axis=0, tiled=True)
-    both = lax.all_gather(along, "tp", axis=0, tiled=False)
+    packed = column_parts(
+        (
+            query_weight,
+            key_weight,
+            value_weight,
+            post_gate_weight,
+            pre_gate_weight,
+            inner_weight,
+            attn_out_weight,
+            conv_out_weight,
+        ),
+        sp,
+    )
+    every, both = gather_all(packed, tokens)
+    every = every.reshape(-1, packed.shape[2])
+    cut = 3 * heads * vsize + 3 * channels
+    into, outof = every[:, :cut], every[:, cut:]
     whole = jnp.concatenate([both[i] for i in range(tp)], axis=1)
     normed = scale_rows(whole.astype(jnp.float32), norm_gain).astype(jnp.bfloat16)
     y = jnp.dot(normed, into, preferred_element_type=jnp.float32)
@@ -228,8 +417,7 @@
     partial = lax.dot_general(
         hidden, outof, (((1,), (1,)), ((), ())), preferred_element_type=jnp.float32
     ).astype(jnp.bfloat16)
-    summed = lax.psum_scatter(partial, "tp", scatter_dimension=0, tiled=True)
-    summed = lax.psum_scatter(summed, "sp", scatter_dimension=0, tiled=True)
+    summed = reduce_all(partial.reshape(tp, sp, -1, partial.shape[1]))
     return summed[None]
 
 
@@ -321,7 +509,8 @@
     def program(*args):
         heads = args[7].shape[0]
         channels = args[12].shape[1]
-        splits = heads % (sp * tp) == 0 and channels % (sp * tp * 128) == 0
+        splits = tp == 2 and mesh.shape["fs"] == 4 and sp > 1 and heads % (sp * tp) == 0
+        splits = splits and channels % (sp * tp * 128) == 0
         return shard(split_device if splits else per_device)(*args)
 
     shard = lambda body: jax.shard_map(

time: 385 us -> 300 us (0.78)
  waiting for transfers between devices: 243 us -> 0 us
  Pallas kernels: 18.2 us -> 251 us
  blocking collectives: 59.2 us -> 0 us
  between operations: 13.8 us -> 0.39 us
  starting transfers between devices: 4.92 us -> 0 us
    pallas_call x0 -> x2, Pallas kernels: none -> 233 us  [the longest x1 128 us: gather_all(): pl.pallas_call(lambda *refs: gather_kernel(n, *refs), out_shape=(jax.Shap...]
    all_gather x4 -> x0, waiting for transfers between devices: 133 us -> none  [the longest x2 88.8 us: gathered_rows(): every = lax.all_gather(mine, 'fs', axis=1, tiled=False)]
    reduce_scatter x2 -> x0, waiting for transfers between devices: 97.1 us -> none  [the longest x1 79.5 us: split_device(): summed = lax.psum_scatter(summed, 'sp', scatter_dimension=0, tiled=True)]
    all_to_all x1 -> x0, blocking collectives: 59.2 us -> none  [gathered_rows(): mine = lax.all_to_all(packed, 'sp', split_axis=0, concat_axis=0, tiled=True)]
    all_to_all x1 -> x0, waiting for transfers between devices: 12.2 us -> none  [gathered_rows(): mine = lax.all_to_all(packed, 'sp', split_axis=0, concat_axis=0, tiled=True)]
    unnamed x37 -> x42, local copies, waits for them, and re-layouts: 4.54 us -> 13.6 us
    all_gather x2 -> x0, local copies, waits for them, and re-layouts: 8.58 us -> none  [gathered_rows(): every = lax.all_gather(mine, 'fs', axis=1, tiled=False)]
    all_to_all x1 -> x0, starting transfers between devices: 4.76 us -> none  [gathered_rows(): mine = lax.all_to_all(packed, 'sp', split_axis=0, concat_axis=0, tiled=True)]
  transfers between devices with their start and end apart: 7 -> 0, of which waited for: 7 -> 0; matrix products, arithmetic and copies ran while one was open for 4% -> 0% of each run, Pallas kernels for 0% -> 0%
where the time goes in v2:
time: 300 us
  Pallas kernels  251 us (84%)
  local copies, waits for them, and re-layouts  22.2 us (7%)
  matrix products  22 us (7%)
  other arithmetic  4.59 us (2%)
    pallas_call x1, Pallas kernels, gather_all(): pl.pallas_call(lambda *refs: gather_kernel(n, *refs), out_shape=(jax.Shap...  128 us
    pallas_call x1, Pallas kernels, reduce_all(): pl.pallas_call(lambda *refs: reduce_kernel(n, *refs), out_shape=jax.Shape...  105 us
    pallas_call x1, Pallas kernels, attention_call(): pl.pallas_call(lambda *refs: attention_kernel(half, *refs), out_shape=jax...  18 us
    dot_general x1, matrix products, split_device(): y = jnp.dot(normed, into, preferred_element_type=jnp.float32)  13.8 us
    unnamed x42, local copies, waits for them, and re-layouts  13.6 us
    dot_general x1, matrix products, split_device(): lax.dot_general(hidden, outof, (((1,), (1,)), ((), ())), preferred_elemen...  8.23 us

profile of v2, /device:TPU:9, one launch (start us, length us, event | category | flops | bytes accessed | tf_op | source)
XLA Modules:
  0.0 300.0 jit_solution(6349274905697022830)
XLA Ops:
  0.0 1.1 copy.16
  1.1 0.1 copy.24
  1.3 1.0 copy.17
  2.3 0.1 copy.25
  2.4 0.0 copy-start.6
  2.5 1.1 copy.18
  3.5 0.1 copy.26
  3.7 0.0 copy-done.4
  3.7 0.2 copy.19
  3.9 0.0 copy-start.8
  3.9 0.1 copy.27
  4.1 0.0 copy-done.5
  4.1 0.0 copy-start.7
  4.1 0.2 copy.20
  4.3 0.1 copy.28
  4.5 0.0 copy-done.6
  4.5 0.2 copy.21
  4.7 0.1 copy.29
  4.9 0.0 copy-done.8
  4.9 0.1 copy.22
  5.0 0.1 copy.30
  5.2 0.2 copy.23
  5.4 0.1 copy.31
  5.5 1.2 copy-done.3
  6.7 127.5 %shard_map.145 = (bf16[4,4,128,1536]{3,2,1,0:T(8,128)(2,1)}, bf16[2,2048,1024]{2,1,0:T(8,128)(2,1)}) custom-call(bf16[4,128,1536]{2,1,0:T(8,128)(2,1)} %bitcast.31, bf16[512,1024]{1,0:T(8,128)(2,1)} %bitcast.33), custom_call_target="tpu_custom_call" | custom-call | tf_op jit(solution)/shard_map/pallas_call | solution.py:275
  134.2 3.9 %slice_bitcast_fusion.1 = (bf16[2048,1024]{1,0:T(8,128)(2,1)S(1)}, bf16[2048,1024]{1,0:T(8,128)(2,1)S(1)}) fusion(bf16[2,2048,1024]{2,1,0:T(8,128)(2,1)} %get-tuple-element.7), kind=kLoop, calls=%fused_computation.12 | loop fusion | bytes 16777216 | tf_op jit(solution)/shard_map/squeeze | solution.py:401
  138.2 0.0 copy-start.9
  138.2 1.9 fusion
  140.1 0.0 copy-done.9
  140.2 13.8 %fusion.3.refs_0_.refs_1_.refs_2_ = f32[2048,1152]{1,0:T(8,128)S(1)} fusion(f32[2048]{0:T(1024)S(1)} %copy-done.9, f32[2048]{0:T(1024)S(1)} %add_rsqrt_fusion, bf16[2048,1024]{1,0:T(8,128)(2,1)S(1)} %get-tuple-element.10, bf16[2048,1024]{1,0:T(8,128)(2,1)S(1)} %get-tuple-element.9, bf16[2048,1536]{1,0:T(8,128)(2,1)} %bitcast.45), kind=kOutput, calls=%fused_computation.5 | convolution fusion | flops 9693036544 | bytes 22560768 | tf_op jit(solution)/shard_map/dot_general | solution.py:403
  154.0 0.2 fusion.8
  154.2 0.2 convert_element_type.28
  154.3 1.1 slice.68
  155.4 3.6 %copy-done = f32[2048,1152]{1,0:T(8,128)} copy-done((f32[2048,1152]{1,0:T(8,128)}, f32[2048,1152]{1,0:T(8,128)S(1)}, u32[]{:S(2)}) %copy-start) | copy-done | bytes 9437208
  159.0 0.9 constant_dynamic-slice_fusion
  159.9 2.1 multiply_convert_fusion
  162.0 0.0 copy-done.10
  162.0 0.1 broadcast_in_dim_tile.6.refs_3_
  162.1 0.1 broadcast_in_dim_tile.7.refs_4_
  162.2 0.6 dynamic_slice.6
  162.8 0.6 broadcast_in_dim.17.refs_5_
  163.4 3.7 %copy-done.1 = f32[2048,1152]{1,0:T(8,128)S(1)} copy-done((f32[2048,1152]{1,0:T(8,128)S(1)}, f32[2048,1152]{1,0:T(8,128)}, u32[]{:S(2)}) %copy-start.1) | copy-done | bytes 9437208
  167.1 18.0 %shard_map.146 = bf16[2048,128]{1,0:T(8,128)(2,1)S(1)} custom-call(f32[2048,1152]{1,0:T(8,128)S(1)} %copy-done.1, f32[2048,1152]{1,0:T(8,128)S(1)} %copy-done.1, f32[2048,1152]{1,0:T(8,128)S(1)} %copy-done.1, f32[1,128]{1,0:T(1,128)S(1)} %broadcast_in_dim_tile.6.refs_3_, f32[1,128]{1,0:T(1,128)S(1)} %broadcast_in_dim_tile.7.refs_4_, ...), custom_call_target="tpu_custom_call" | custom-call | flops 4294967296 | bytes 3670016 | tf_op jit(solution)/shard_map/pallas_call | solution.py:131
  185.1 0.2 pad_maximum_fusion.2
  185.3 0.2 copy.32
  185.5 8.2 %convolution_convert_fusion = bf16[2048,2048]{1,0:T(8,128)(2,1)} fusion(bf16[2048,384]{1,0:T(8,128)(2,1)S(1)} %bitcast.32, bf16[2048,1536]{1,0:T(8,128)(2,1)} %bitcast.46), kind=kOutput, calls=%fused_computation.9 | convolution fusion | flops 3225419776 | bytes 11534336 | tf_op jit(solution)/shard_map/dot_general | solution.py:417
  193.7 105.3 %shard_map.147 = bf16[256,2048]{1,0:T(8,128)(2,1)S(1)} custom-call(bf16[2,4,256,2048]{3,2,1,0:T(8,128)(2,1)} %bitcast.29), custom_call_target="tpu_custom_call" | custom-call | tf_op jit(solution)/shard_map/pallas_call | solution.py:342
  299.0 1.0 copy.41
  (24 shorter events, 0.2 us)
Async XLA Ops:
  0.0 3.7 %copy-start.4 = (bf16[128,1024]{1,0:T(8,128)(2,1)S(1)}, bf16[128,1024]{1,0:T(8,128)(2,1)}, u32[]{:S(2)}) copy-start(bf16[128,1024]{1,0:T(8,128)(2,1)} %param.24) | copy-start | bytes 786436
  0.0 4.1 %copy-start.5 = (bf16[128,1024]{1,0:T(8,128)(2,1)S(1)}, bf16[128,1024]{1,0:T(8,128)(2,1)}, u32[]{:S(2)}) copy-start(bf16[128,1024]{1,0:T(8,128)(2,1)} %param.25) | copy-start | bytes 786436
  2.4 2.1 copy-start.6
  3.9 0.9 copy-start.8
  4.1 1.1 copy-start.7
  5.5 1.2 copy-start.3
  138.2 2.0 copy-start.9
  155.4 3.6 %copy-start = (f32[2048,1152]{1,0:T(8,128)}, f32[2048,1152]{1,0:T(8,128)S(1)}, u32[]{:S(2)}) copy-start(f32[2048,1152]{1,0:T(8,128)S(1)} %fusion.3.refs_0_.refs_1_.refs_2_) | copy-start | bytes 28311556
  159.9 2.1 copy-start.10
  159.9 2.2 copy-start.11
  159.9 2.3 copy-start.12
  159.9 3.5 %copy-start.2 = (f32[128]{0:T(128)S(1)}, f32[128]{0:T(128)}, u32[]{:S(2)}) copy-start(f32[128]{0:T(128)} %param.23) | copy-start | bytes 1540
  163.4 3.7 %copy-start.1 = (f32[2048,1152]{1,0:T(8,128)S(1)}, f32[2048,1152]{1,0:T(8,128)}, u32[]{:S(2)}) copy-start(f32[2048,1152]{1,0:T(8,128)} %copy-done) | copy-start | bytes 28311556

commit v3 on v2

--- a/solution.py
+++ b/solution.py
@@ -236,11 +236,21 @@
         go(remote(w_all.at[s, held], w_all.at[s, held], g_send.at[d], g_recv.at[d], {"fs": to}))
 
     spread(0, w_ref.at[z])
-    tokens = {
-        d: go(remote(t_ref, place(z), t_send.at[d], t_recv.at[d], {"sp": (z + d) % n}))
-        for d in near
-    }
-    go(remote(t_ref, place(z), p_send.at[0], p_recv.at[0], {"tp": 1 - c}))
+    def along(source, s, step):
+        return remote(source, place(s), t_send.at[(step + 1) // 2, s], t_recv.at[s], {"sp": z + step})
+
+    def aside(source, s):
+        return remote(source, place(s), p_send.at[s], p_recv.at[s], {"tp": 1 - c})
+
+    @pl.when(z + 1 < n)
+    def _():
+        along(t_ref, z, 1).start()
+
+    @pl.when(z > 0)
+    def _():
+        along(t_ref, z, -1).start()
+
+    aside(t_ref, z).start()
     mine = [
         pltpu.make_async_copy(w_ref.at[z], w_all.at[z, f], own.at[0]),
         pltpu.make_async_copy(t_ref, place(z), own.at[1]),
@@ -254,11 +264,35 @@
         pass_on(last)
         last = d
     pass_on(last)
-    for d in near:
-        tokens[d].wait_recv()
-        s = (z + n - d) % n
-        go(remote(place(s), place(s), p_send.at[d], p_recv.at[d], {"tp": 1 - c}))
-    waited = set(map(id, across.values())) | set(map(id, tokens.values()))
+    for k in range(1, n):
+        for step in (1, -1):
+            s = z - step * k
+
+            @pl.when(jnp.logical_and(s >= 0, s < n))
+            def _(s=s, step=step):
+                along(place(s), s, step).wait_recv()
+
+                @pl.when(jnp.logical_and(z + step >= 0, z + step < n))
+                def _():
+                    along(place(s), s, step).start()
+
+                aside(place(s), s).start()
+
+    for k in range(n):
+        for step in (1, -1) if k else (1,):
+            s = z - step * k
+
+            @pl.when(jnp.logical_and(s >= 0, s < n))
+            def _(s=s, step=step, k=k):
+                for way in (step,) if k else (1, -1):
+                    @pl.when(jnp.logical_and(z + way >= 0, z + way < n))
+                    def _(way=way):
+                        along(place(s), s, way).wait_send()
+
+                aside(place(s), s).wait_send()
+                aside(place(s), s).wait_recv()
+
+    waited = set(map(id, across.values()))
     waited |= {id(side[d % 2, d]) for d in range(n)}
     for copy in flights:
         copy.wait_send()
@@ -282,7 +316,7 @@
         out_specs=(pl.BlockSpec(memory_space=pl.ANY),) * 2,
         scratch_shapes=[
             dma((2,)), dma((n,)), dma((n,)), dma((2, n)), dma((2, n)), dma((n,)), dma((n,)),
-            dma((n,)), dma((n,)), dma((n,)), dma((n,)),
+            dma((2, n)), dma((n,)), dma((n,)), dma((n,)),
         ],
         compiler_params=pltpu.CompilerParams(collective_id=1, has_side_effects=True),
     )(packed, tokens)

time: 300 us -> 279 us (0.930)
  Pallas kernels: 251 us -> 229 us
    pallas_call x1, Pallas kernels: 128 us -> 104 us  [gather_all(): pl.pallas_call(lambda *refs: gather_kernel(n, *refs), out_shape=(jax.Shap...]
where the time goes in v3:
time: 279 us; the launch traced here: 278 us
  Pallas kernels  229 us (82%)
  local copies, waits for them, and re-layouts  22.2 us (8%)
  matrix products  22 us (8%)
  other arithmetic  4.59 us (2%)
    pallas_call x1, Pallas kernels, reduce_all(): pl.pallas_call(lambda *refs: reduce_kernel(n, *refs), out_shape=jax.Shape...  107 us
    pallas_call x1, Pallas kernels, gather_all(): pl.pallas_call(lambda *refs: gather_kernel(n, *refs), out_shape=(jax.Shap...  104 us
    pallas_call x1, Pallas kernels, attention_call(): pl.pallas_call(lambda *refs: attention_kernel(half, *refs), out_shape=jax...  18 us
    dot_general x1, matrix products, split_device(): y = jnp.dot(normed, into, preferred_element_type=jnp.float32)  13.8 us
    unnamed x42, local copies, waits for them, and re-layouts  13.6 us
    dot_general x1, matrix products, split_device(): lax.dot_general(hidden, outof, (((1,), (1,)), ((), ())), preferred_elemen...  8.23 us

profile of v3, /device:TPU:9, one launch (start us, length us, event | category | flops | bytes accessed | tf_op | source)
XLA Modules:
  0.0 278.4 jit_solution(1288530210660851743)
XLA Ops:
  0.0 1.1 copy.16
  1.1 0.1 copy.24
  1.3 1.0 copy.17
  2.3 0.1 copy.25
  2.4 0.0 copy-start.6
  2.5 1.1 copy.18
  3.5 0.1 copy.26
  3.7 0.0 copy-done.4
  3.7 0.2 copy.19
  3.9 0.0 copy-start.8
  3.9 0.1 copy.27
  4.1 0.0 copy-done.5
  4.1 0.0 copy-start.7
  4.1 0.2 copy.20
  4.3 0.1 copy.28
  4.5 0.0 copy-done.6
  4.5 0.2 copy.21
  4.7 0.1 copy.29
  4.9 0.0 copy-done.8
  4.9 0.1 copy.22
  5.0 0.1 copy.30
  5.2 0.0 copy-done.7
  5.2 0.2 copy.23
  5.4 0.1 copy.31
  5.5 1.2 copy-done.3
  6.7 103.8 %shard_map.145 = (bf16[4,4,128,1536]{3,2,1,0:T(8,128)(2,1)}, bf16[2,2048,1024]{2,1,0:T(8,128)(2,1)}) custom-call(bf16[4,128,1536]{2,1,0:T(8,128)(2,1)} %bitcast.31, bf16[512,1024]{1,0:T(8,128)(2,1)} %bitcast.33), custom_call_target="tpu_custom_call" | custom-call | tf_op jit(solution)/shard_map/pallas_call | solution.py:309
  110.6 3.9 %slice_bitcast_fusion.1 = (bf16[2048,1024]{1,0:T(8,128)(2,1)S(1)}, bf16[2048,1024]{1,0:T(8,128)(2,1)S(1)}) fusion(bf16[2,2048,1024]{2,1,0:T(8,128)(2,1)} %get-tuple-element.7), kind=kLoop, calls=%fused_computation.12 | loop fusion | bytes 16777216 | tf_op jit(solution)/shard_map/squeeze | solution.py:435
  114.5 0.0 copy-start.9
  114.5 1.9 fusion
  116.5 13.8 %fusion.3.refs_0_.refs_1_.refs_2_ = f32[2048,1152]{1,0:T(8,128)S(1)} fusion(f32[2048]{0:T(1024)S(1)} %copy-done.9, f32[2048]{0:T(1024)S(1)} %add_rsqrt_fusion, bf16[2048,1024]{1,0:T(8,128)(2,1)S(1)} %get-tuple-element.10, bf16[2048,1024]{1,0:T(8,128)(2,1)S(1)} %get-tuple-element.9, bf16[2048,1536]{1,0:T(8,128)(2,1)} %bitcast.45), kind=kOutput, calls=%fused_computation.5 | convolution fusion | flops 9693036544 | bytes 22560768 | tf_op jit(solution)/shard_map/dot_general | solution.py:437
  130.3 0.2 fusion.8
  130.5 0.2 convert_element_type.28
  130.7 1.1 slice.68
  131.8 3.6 %copy-done = f32[2048,1152]{1,0:T(8,128)} copy-done((f32[2048,1152]{1,0:T(8,128)}, f32[2048,1152]{1,0:T(8,128)S(1)}, u32[]{:S(2)}) %copy-start) | copy-done | bytes 9437208
  135.4 0.9 constant_dynamic-slice_fusion
  136.3 2.1 multiply_convert_fusion
  138.4 0.1 broadcast_in_dim_tile.6.refs_3_
  138.4 0.1 broadcast_in_dim_tile.7.refs_4_
  138.5 0.0 copy-done.12
  138.5 0.6 dynamic_slice.6
  139.1 0.6 broadcast_in_dim.17.refs_5_
  139.8 3.7 %copy-done.1 = f32[2048,1152]{1,0:T(8,128)S(1)} copy-done((f32[2048,1152]{1,0:T(8,128)S(1)}, f32[2048,1152]{1,0:T(8,128)}, u32[]{:S(2)}) %copy-start.1) | copy-done | bytes 9437208
  143.5 18.0 %shard_map.146 = bf16[2048,128]{1,0:T(8,128)(2,1)S(1)} custom-call(f32[2048,1152]{1,0:T(8,128)S(1)} %copy-done.1, f32[2048,1152]{1,0:T(8,128)S(1)} %copy-done.1, f32[2048,1152]{1,0:T(8,128)S(1)} %copy-done.1, f32[1,128]{1,0:T(1,128)S(1)} %broadcast_in_dim_tile.6.refs_3_, f32[1,128]{1,0:T(1,128)S(1)} %broadcast_in_dim_tile.7.refs_4_, ...), custom_call_target="tpu_custom_call" | custom-call | flops 4294967296 | bytes 3670016 | tf_op jit(solution)/shard_map/pallas_call | solution.py:131
  161.5 0.2 pad_maximum_fusion.2
  161.7 0.2 copy.32
  161.9 8.2 %convolution_convert_fusion = bf16[2048,2048]{1,0:T(8,128)(2,1)} fusion(bf16[2048,384]{1,0:T(8,128)(2,1)S(1)} %bitcast.32, bf16[2048,1536]{1,0:T(8,128)(2,1)} %bitcast.46), kind=kOutput, calls=%fused_computation.9 | convolution fusion | flops 3225419776 | bytes 11534336 | tf_op jit(solution)/shard_map/dot_general | solution.py:451
  170.1 107.3 %shard_map.147 = bf16[256,2048]{1,0:T(8,128)(2,1)S(1)} custom-call(bf16[2,4,256,2048]{3,2,1,0:T(8,128)(2,1)} %bitcast.29), custom_call_target="tpu_custom_call" | custom-call | tf_op jit(solution)/shard_map/pallas_call | solution.py:376
  277.4 1.0 copy.41
  (24 shorter events, 0.2 us)
Async XLA Ops:
  0.0 3.7 %copy-start.4 = (bf16[128,1024]{1,0:T(8,128)(2,1)S(1)}, bf16[128,1024]{1,0:T(8,128)(2,1)}, u32[]{:S(2)}) copy-start(bf16[128,1024]{1,0:T(8,128)(2,1)} %param.24) | copy-start | bytes 786436
  0.0 4.1 %copy-start.5 = (bf16[128,1024]{1,0:T(8,128)(2,1)S(1)}, bf16[128,1024]{1,0:T(8,128)(2,1)}, u32[]{:S(2)}) copy-start(bf16[128,1024]{1,0:T(8,128)(2,1)} %param.25) | copy-start | bytes 786436
  2.4 2.1 copy-start.6
  3.9 0.9 copy-start.8
  4.1 1.1 copy-start.7
  5.5 1.2 copy-start.3
  114.5 2.0 copy-start.9
  131.8 3.6 %copy-start = (f32[2048,1152]{1,0:T(8,128)}, f32[2048,1152]{1,0:T(8,128)S(1)}, u32[]{:S(2)}) copy-start(f32[2048,1152]{1,0:T(8,128)S(1)} %fusion.3.refs_0_.refs_1_.refs_2_) | copy-start | bytes 28311556
  136.3 2.1 copy-start.10
  136.3 2.2 copy-start.11
  136.3 2.3 copy-start.12
  136.3 3.5 %copy-start.2 = (f32[128]{0:T(128)S(1)}, f32[128]{0:T(128)}, u32[]{:S(2)}) copy-start(f32[128]{0:T(128)} %param.23) | copy-start | bytes 1540
  139.8 3.7 %copy-start.1 = (f32[2048,1152]{1,0:T(8,128)S(1)}, f32[2048,1152]{1,0:T(8,128)}, u32[]{:S(2)}) copy-start(f32[2048,1152]{1,0:T(8,128)} %copy-done) | copy-start | bytes 28311556
